TPU v7x, 32 devices: a whole 2x2x4 slice. The times are simulated.
32 devices in a mesh: gr: 2 (over core), sp: 8 (over z, y), tp: 2 (over x).
Axes of the slice: x: 2, y: 2, z: 4, core: 2. Of those that a mesh axis runs over, the one named last changes fastest.
Arguments:
- tokens: bfloat16 [4, 2048, 2048], P('gr', ('sp', 'tp')), parts along dimension 0, may hold values from -6 to 6
- key_weight: bfloat16 [2048, 1024], P('sp'), may hold values from -0.125 to 0.125
- value_weight: bfloat16 [2048, 1024], P('sp'), may hold values from -0.125 to 0.125
- queries: bfloat16 [4, 1024], P('gr'), parts along dimension 0, may hold values from -6 to 6
- head_offset: float32 [16], replicated, may hold values from -14 to -3.5
- key_bias: bfloat16 [4, 2048, 16], P('gr', ('sp', 'tp')), parts along dimension 0, may hold values from -0.5 to 12.9
Outputs:
- key_cache: bfloat16 [4, 2048, 1024], P('gr', 'sp', 'tp'), parts along dimension 0
- value_cache: bfloat16 [4, 2048, 1024], P('gr', 'sp', 'tp'), parts along dimension 0
- bias_cache: bfloat16 [4, 2048, 16], P('gr', 'sp', 'tp'), parts along dimension 0
- reading: float32 [4, 1024], P('gr', 'tp'), parts along dimension 0
There are 2 independent parts, one for each index of `gr`. A program takes and returns all parts, laid end to end along the dimension named above; an argument that names none is the same for every part. Nothing has to cross between parts.
All inputs are finite; a program needn't handle non-finite values.
Results may differ from a plain program's by a relative error of at most 0.0052.
Values may be sent and summed in bfloat16 or wider, within the bound.
A program may use at most 64 MiB of HBM per device.

v0:
```python
import jax
import jax.numpy as jnp
from jax import lax
from jax.sharding import PartitionSpec as P


def carried_in(x, axis, combine, identity):
    length, position = (lax.axis_size(axis), lax.axis_index(axis))
    everything = lax.all_gather(x, axis)
    start = jnp.broadcast_to(jnp.asarray(identity, x.dtype), x.shape)

    def lap(k, before):
        at = length - 1 - k
        reached = at > position
        new = combine(before, everything[at])
        return jnp.where(reached, new, before)

    return lax.fori_loop(0, length, lap, start)


def add_terms(earlier, later):
    return earlier + later


def normalize(mixture):
    return mixture * lax.rsqrt(jnp.mean(mixture * mixture, axis=-1, keepdims=True) + 1e-06)


def per_device(tokens, key_weight, value_weight, queries, head_offset, key_bias):
    seq_count, pos_dev, model_width = tokens.shape
    head_count = head_offset.shape[0]
    kv_width = key_weight.shape[1]
    head_dim = kv_width // head_count
    score_scale = head_dim ** (-0.5)
    tp_count = lax.axis_size("tp")
    col_width = kv_width // tp_count
    col_start = lax.axis_index("tp") * col_width
    own_cols = jnp.concatenate(
        [
            lax.dynamic_slice_in_dim(key_weight, col_start, col_width, 1),
            lax.dynamic_slice_in_dim(value_weight, col_start, col_width, 1),
        ],
        axis=1,
    )
    full_cols = lax.all_gather(own_cols, "sp", axis=0, tiled=True)
    projected = jnp.einsum(
        "spd,dw->spw",
        lax.all_gather(tokens, "tp", axis=1, tiled=True),
        full_cols,
        preferred_element_type=jnp.float32,
    ).astype(jnp.bfloat16)
    key_cache = projected[:, :, :col_width]
    value_cache = projected[:, :, col_width:]
    bias_cache = lax.all_to_all(key_bias, "tp", split_axis=2, concat_axis=1, tiled=True)
    span_len = key_cache.shape[1]
    local_heads = bias_cache.shape[2]
    key_blocks = key_cache.reshape(seq_count, span_len, local_heads, head_dim)
    value_blocks = value_cache.reshape(seq_count, span_len, local_heads, head_dim)
    query_cols = lax.dynamic_slice_in_dim(queries, col_start, col_width, 1)
    query_heads = query_cols.reshape(seq_count, local_heads, head_dim)
    head_start = lax.axis_index("tp") * local_heads
    local_offset = lax.dynamic_slice_in_dim(head_offset, head_start, local_heads, 0)
    logits = (
        jnp.einsum("sphc,shc->shp", key_blocks, query_heads, preferred_element_type=jnp.float32)
        * score_scale
    )
    logits = (
        logits
        + local_offset[None, :, None]
        + jnp.transpose(bias_cache.astype(jnp.float32), (0, 2, 1))
    )
    fading = jax.nn.log_sigmoid(-logits)
    within = lax.cumsum(fading, axis=2, reverse=True) - fading
    block_total = jnp.sum(fading, axis=2)
    carried = carried_in(block_total, "sp", add_terms, jnp.zeros_like(block_total))
    weights = jnp.exp(jax.nn.log_sigmoid(logits) + within + carried[:, :, None]).astype(
        jnp.bfloat16
    )
    partial_value = jnp.einsum(
        "shp,sphc->shc", weights, value_blocks, preferred_element_type=jnp.float32
    )
    mixture = lax.psum(partial_value, "sp")
    reading = normalize(mixture).reshape(seq_count, col_width)
    return (key_cache, value_cache, bias_cache, reading)


def solution(mesh):
    in_specs = (
        P("gr", ("sp", "tp"), None),
        P("sp", None),
        P("sp", None),
        P("gr", None),
        P(),
        P("gr", ("sp", "tp"), None),
    )
    out_specs = (P("gr", "sp", "tp"), P("gr", "sp", "tp"), P("gr", "sp", "tp"), P("gr", "tp"))
    return jax.shard_map(
        per_device, mesh=mesh, in_specs=in_specs, out_specs=out_specs, check_vma=False
    )
```

profile of v0, /device:TPU:0, one launch (start us, length us, event | category | flops | bytes accessed | tf_op | source)
XLA Modules:
  0.0 179.6 jit_solution(294673093222609058)
XLA Ops:
  7.2 0.0 copy-start
  7.2 0.0 all-gather.7.cloned.1.call-start
  7.2 0.7 all-gather.7.cloned.1.call-update
  7.9 0.0 copy-start.2
  7.9 0.0 copy-start.3
  7.9 0.0 all-gather.5.cloned.1.call-start
  8.0 1.1 constant_dynamic-slice_fusion.1
  9.1 0.1 copy.28
  9.2 0.1 copy.29
  9.3 0.8 pad_maximum_fusion
  10.2 0.0 all-gather.5.cloned.1.call-update
  10.2 0.0 copy-done.2
  10.2 0.6 copy.20
  10.8 4.2 %all-to-all-start = ((bf16[2,128,16]{1,0,2:T(2,128)(2,1)}), bf16[2,128,16]{1,0,2:T(2,128)(2,1)S(1)}, u32[]{:S(2)}, u32[]{:S(2)}) async-start(bf16[2,128,16]{1,0,2:T(2,128)(2,1)} %copy.20), calls=%async_computation | async-start | bytes 16384 | tf_op jit(solution)/shard_map/all_to_all | solution.py:54
  15.0 0.0 copy-done
  15.1 0.1 reshape.64
  15.1 0.0 copy-done.3
  15.1 0.1 dynamic_slice.25
  15.2 30.2 %all-gather.7.cloned.1.call-done = bf16[2,256,2048]{2,1,0:T(8,128)(2,1)} async-done(((bf16[2,128,2048]{2,1,0:T(8,128)(2,1)}), bf16[2,256,2048]{2,1,0:T(8,128)(2,1)}) %all-gather.7.cloned.1.call-update) | async-done | bytes 2097168 | tf_op jit(solution)/shard_map/all_gather | solution.py:48
  45.4 77.3 %all-gather.5.cloned.1.call-done = bf16[2048,1024]{0,1:T(8,128)(2,1)} async-done(((bf16[256,1024]{0,1:T(8,128)(2,1)}), bf16[2048,1024]{0,1:T(8,128)(2,1)}) %all-gather.5.cloned.1.call-update) | async-done | bytes 4194320 | tf_op jit(solution)/shard_map/all_gather | solution.py:45
  122.7 5.2 %fusion.5 = bf16[2,256,1024]{1,2,0:T(8,128)(2,1)S(1)} fusion(bf16[2,256,2048]{2,1,0:T(8,128)(2,1)} %all-gather.7.cloned.1.call-done, bf16[2048,1024]{0,1:T(8,128)(2,1)} %all-gather.5.cloned.1.call-done), kind=kOutput, calls=%fused_computation.4 | convolution fusion | flops 2148007936 | bytes 7340032 | tf_op jit(solution)/shard_map/spd,dw->spw/dot_general | solution.py:46
  127.9 0.1 fusion.18
  128.0 0.2 fusion.19
  128.2 1.0 copy.22
  129.2 0.0 all-to-all-done
  129.2 0.1 negate_bitcast_fusion
  129.3 0.0 copy-start.1
  129.3 0.2 fusion.16
  129.5 17.7 %all-gather.1 = f32[8,2,8]{2,1,0:T(2,128)S(1)} all-gather(f32[1,2,8]{2,1,0:T(2,128)S(1)} %negate_bitcast_fusion.1), channel_id=2, replica_groups=mesh['gr'=2,'sp'=8,'tp'=2] {'sp'}, dimensions={0}, use_global_device_ids=true | all-gather | bytes 576 | tf_op jit(solution)/shard_map/all_gather | solution.py:9
  147.2 0.3 while.16
  147.5 5.0 %reduce-window.6 = f32[2,8,2,128]{3,1,2,0:T(8,128)S(1)} reduce-window(f32[2,8,2,128]{3,1,2,0:T(8,128)S(1)} %get-tuple-element.150, f32[]{:T(128)} %constant.72.clone.1), window={size=1x1x1x128 pad=0_0x0_0x0_0x0_127}, to_apply=%region_0.1 | reduce-window | flops 520192 | bytes 32772 | tf_op jit(solution)/shard_map/reduce-window
  152.5 0.1 slice_reduce_fusion
  152.6 1.0 copy.23
  153.6 0.1 fusion.17
  153.7 0.2 fusion.14
  153.9 17.9 %psum.7 = f32[2,8,64]{2,1,0:T(8,128)S(1)} all-reduce(f32[2,8,64]{2,1,0:T(8,128)S(1)} %bitcast.62), channel_id=1, replica_groups=mesh['gr'=2,'sp'=8,'tp'=2] {'sp'}, use_global_device_ids=true, to_apply=%region_5.6 | all-reduce | flops 1024 | bytes 8192 | tf_op jit(solution)/shard_map/psum | solution.py:82
  171.9 0.1 multiply_reduce_fusion
  172.0 0.1 broadcast_multiply_fusion
  172.1 0.7 reshape.53
  172.7 0.0 copy-done.1
  (14 shorter events, 0.2 us)
Async XLA Ops:
  7.2 7.9 %copy-start = (bf16[2,1024]{1,0:T(2,128)(2,1)S(1)}, bf16[2,1024]{1,0:T(2,128)(2,1)}, u32[]{:S(2)}) copy-start(bf16[2,1024]{1,0:T(2,128)(2,1)} %param.11) | copy-start | bytes 12292
  7.2 38.2 %all-gather.7.cloned.1.call-start = ((), (), s32[]{:S(2)}) async-start(), calls=%async_computation.2 | async-start | bytes 3145728 | tf_op jit(solution)/shard_map/all_gather | solution.py:48
  7.9 2.3 %copy-start.2 = (bf16[2,128,16]{1,2,0:T(8,128)(2,1)S(1)}, bf16[2,128,16]{1,2,0:T(8,128)(2,1)}, u32[]{:S(2)}) copy-start(bf16[2,128,16]{1,2,0:T(8,128)(2,1)} %param.13) | copy-start | bytes 24580
  7.9 7.2 %copy-start.3 = (f32[16]{0:T(128)S(1)}, f32[16]{0:T(128)}, u32[]{:S(2)}) copy-start(f32[16]{0:T(128)} %param.12) | copy-start | bytes 196
  7.9 114.7 %all-gather.5.cloned.1.call-start = ((), (), s32[]{:S(2)}) async-start(), calls=%async_computation.1 | async-start | bytes 4718592 | tf_op jit(solution)/shard_map/all_gather | solution.py:45
  10.8 118.4 %all-to-all-start = ((bf16[2,128,16]{1,0,2:T(2,128)(2,1)}), bf16[2,128,16]{1,0,2:T(2,128)(2,1)S(1)}, u32[]{:S(2)}, u32[]{:S(2)}) async-start(bf16[2,128,16]{1,0,2:T(2,128)(2,1)} %copy.20), calls=%async_computation | async-start | bytes 16384 | tf_op jit(solution)/shard_map/all_to_all | solution.py:54
  129.3 43.5 %copy-start.1 = (bf16[2,256,8]{1,2,0:T(8,128)(2,1)}, bf16[2,256,8]{1,2,0:T(8,128)(2,1)S(1)}, u32[]{:S(2)}) copy-start(bf16[2,256,8]{1,2,0:T(8,128)(2,1)S(1)} %get-tuple-element.151) | copy-start | bytes 24580
Sparse Core Ops, SparseCore 0:
  9.5 35.8 all-gather.6
  48.0 74.6 all-gather.4
where the time goes:
time: 180 us
  waiting for transfers between devices  108 us (60%)
  blocking collectives  35.7 us (20%)
  between operations  14.2 us (8%)
  other arithmetic  6.49 us (4%)
  matrix products  5.64 us (3%)
  local copies, waits for them, and re-layouts  4.99 us (3%)
  starting transfers between devices  4.31 us (2%)
    all_gather x1, waiting for transfers between devices, per_device(): full_cols = lax.all_gather(own_cols, 'sp', axis=0, tiled=True)  77.3 us
    all_gather x1, waiting for transfers between devices, per_device(): lax.all_gather(tokens, 'tp', axis=1, tiled=True)  30.2 us
    psum x1, blocking collectives, per_device(): mixture = lax.psum(partial_value, 'sp')  17.9 us
    all_gather x1, blocking collectives, carried_in(): everything = lax.all_gather(x, axis)  17.7 us
    dot_general x1, matrix products, per_device(): jnp.einsum('spd,dw->spw', lax.all_gather(tokens, 'tp', axis=1, tiled=True...  5.22 us
    another operation x2, other arithmetic  5.02 us
    all_to_all x1, starting transfers between devices, per_device(): lax.all_to_all(key_bias, 'tp', split_axis=2, concat_axis=1, tiled=True)  4.23 us
  transfers between devices with their start and end apart: 3, of which 2 were waited for; matrix products, arithmetic and copies ran while one was open for 5% of the time, Pallas kernels for 0%

commit v1 on v0

v1 whole, which is shorter than its diff:
```python
import functools

import jax
import jax.numpy as jnp
from jax import lax
from jax.experimental import pallas as pl
from jax.experimental.pallas import tpu as pltpu
from jax.sharding import PartitionSpec as P

MESH = pl.DeviceIdType.MESH
F32 = jnp.float32
BF16 = jnp.bfloat16
SUBS = 2


def ring_place(index, length):
    lane, row = lax.rem(index, 2), index // 2
    return row * (1 - lane) + (length - 1 - row) * lane


def ring_index(place, length):
    lane = place // (length // 2)
    row = place * (1 - lane) + (length - 1 - place) * lane
    return 2 * row + lane


def kernel(
    dims,
    tokens, key_weight, value_weight, queries, head_offset, key_bias,
    key_out, value_out, bias_out, reading_out,
    tok, wts, acc, kv, bias, query, offset, bias_all, packed,
    local_sem, ring_send, ring_recv, pair_send, pair_recv,
    tok_send, tok_recv, bias_send, bias_recv, mix_send, mix_recv, out_sem,
):
    n, tp_count, seqs, pos, width, rows, cols, heads, head_dim, rows_h = dims
    hops = n // 2
    sub_rows = rows // SUBS
    span = tp_count * pos
    me, tp, gr = lax.axis_index("sp"), lax.axis_index("tp"), lax.axis_index("gr")
    place = ring_place(me, n)

    def owner_at(step):
        return ring_index(lax.rem(place + step + n, n), n)

    right, left = owner_at(1), owner_at(-1)
    partner = 1 - gr
    col_start = pl.multiple_of(tp * cols, 128)
    chunked = (width // n) % 128 == 0
    order = [0]
    for h in range(1, hops + 1):
        order.extend([-h, h] if h < hops else [h])
    chunk = width // n if chunked else width
    my_rows = pl.ds(pl.multiple_of(tp * pos, pos), pos)

    weight_copies = [
        pltpu.make_async_copy(
            w.at[:, pl.ds(col_start, cols)], wts.at[part, me], local_sem.at[part]
        )
        for part, w in enumerate((key_weight, value_weight))
    ]
    tok_copy = pltpu.make_async_copy(tokens, tok.at[:, my_rows, :], local_sem.at[2])
    bias_copy = pltpu.make_async_copy(key_bias, bias_all, local_sem.at[3])
    query_copy = pltpu.make_async_copy(queries, query, local_sem.at[4])
    offset_copy = pltpu.make_async_copy(head_offset, offset, local_sem.at[5])
    for c in (*weight_copies, tok_copy, bias_copy, query_copy, offset_copy):
        c.start()

    tp_peers = [lax.rem(tp + k, tp_count) for k in range(1, tp_count)]
    barrier = pltpu.get_barrier_semaphore()
    for target in ({"sp": right}, {"sp": left}, {"gr": partner}, *({"tp": p} for p in tp_peers)):
        pl.semaphore_signal(barrier, inc=1, device_id=target, device_id_type=MESH)

    def ring_copy(direction, hop, sub, step):
        block = wts.at[gr, owner_at(step), pl.ds(sub * sub_rows, sub_rows), :]
        return pltpu.make_async_remote_copy(
            src_ref=block, dst_ref=block,
            send_sem=ring_send.at[direction, hop - 1, sub],
            recv_sem=ring_recv.at[direction, hop - 1, sub],
            device_id={"sp": right if direction == 0 else left}, device_id_type=MESH,
        )

    def step_of(direction, hop):
        return -hop if direction == 0 else hop

    def sent(direction, hop, sub):
        return ring_copy(direction, hop, sub, step_of(direction, hop - 1))

    def got(direction, hop, sub):
        return ring_copy(direction, hop, sub, step_of(direction, hop))

    def used(direction, hop, sub):
        return hop < hops or (hop == hops and sub % 2 == direction)

    def pair_copy(direction, hop, sub, part):
        block = wts.at[part, owner_at(step_of(direction, hop)), pl.ds(sub * sub_rows, sub_rows), :]
        return pltpu.make_async_remote_copy(
            src_ref=block, dst_ref=block,
            send_sem=pair_send.at[direction, hop - 1, sub],
            recv_sem=pair_recv.at[direction, hop - 1, sub],
            device_id={"gr": partner}, device_id_type=MESH,
        )

    def tok_columns(i):
        if not chunked:
            return pl.ds(0, width)
        return pl.ds(pl.multiple_of(owner_at(order[i]) * chunk, 128), chunk)

    chunk_count = len(order) if chunked else 1

    def tok_move(i, k, source):
        place_rows = pl.ds(pl.multiple_of(source * pos, pos), pos)
        block = tok.at[:, place_rows, tok_columns(i)]
        return pltpu.make_async_remote_copy(
            src_ref=block, dst_ref=block,
            send_sem=tok_send.at[i, k], recv_sem=tok_recv.at[i, k],
            device_id={"tp": lax.rem(tp + k + 1, tp_count)}, device_id_type=MESH,
        )

    def bias_move(k, source, target):
        return pltpu.make_async_remote_copy(
            src_ref=bias_all.at[:, target], dst_ref=bias.at[source],
            send_sem=bias_send.at[k], recv_sem=bias_recv.at[k],
            device_id={"tp": lax.rem(tp + k + 1, tp_count)}, device_id_type=MESH,
        )

    pl.semaphore_wait(barrier, 3 + len(tp_peers))
    for c in weight_copies:
        c.wait()
    sent_list = []

    def launch(c):
        c.start()
        sent_list.append(c)

    for sub in range(SUBS):
        for direction in range(2):
            if used(direction, 1, sub):
                launch(sent(direction, 1, sub))
    tok_copy.wait()
    for i in range(chunk_count):
        for k in range(tp_count - 1):
            launch(tok_move(i, k, tp))
    bias_copy.wait()
    for k in range(tp_count - 1):
        launch(bias_move(k, tp, lax.rem(tp + k + 1, tp_count)))
    query_copy.wait()
    offset_copy.wait()

    def tokens_ready(i):
        for k in range(tp_count - 1):
            tok_move(i, k, lax.rem(tp + tp_count - k - 1, tp_count)).wait_recv()

    def multiply(i, last):
        owner = owner_at(order[i])
        for part in range(2):
            w = wts[part, owner]

            def body(s, carry):
                x = tok[s, :, tok_columns(i)]
                y = jnp.dot(x, w, preferred_element_type=F32)
                if i > 0:
                    y = acc[part, s] + y
                if last:
                    kv[part, s] = y.astype(BF16)
                else:
                    acc[part, s] = y
                return carry

            lax.fori_loop(0, seqs, body, 0)
            if last:
                pltpu.make_async_copy(
                    kv.at[part], (key_out, value_out)[part], out_sem.at[part]
                ).start()

    def pair_ready(hop):
        for direction in range(2):
            for sub in range(SUBS):
                if used(direction, hop, sub):
                    pair_copy(direction, hop, sub, partner).wait_recv()

    def steps_of_hop(hop):
        if hop == 0:
            return [0]
        first = 1 + 2 * (hop - 1)
        return [first, first + 1] if hop < hops else [first]

    def compute_hop(hop):
        if hop > 0:
            pair_ready(hop)
        if chunked:
            for i in steps_of_hop(hop):
                tokens_ready(i)
                multiply(i, i == len(order) - 1)

    for hop in range(1, hops + 1):
        for sub in range(SUBS):
            for direction in range(2):
                if not used(direction, hop, sub):
                    continue
                got(direction, hop, sub).wait_recv()
                if hop < hops and used(direction, hop + 1, sub):
                    launch(sent(direction, hop + 1, sub))
                launch(pair_copy(direction, hop, sub, gr))
        compute_hop(hop - 1)
    compute_hop(hops)

    if not chunked:
        tokens_ready(0)
        tile = pos
        for part in range(2):
            w = wts[part].reshape(width, cols)

            def body(j, carry):
                s, r = j // (span // tile), lax.rem(j, span // tile)
                where = pl.ds(pl.multiple_of(r * tile, tile), tile)
                y = jnp.dot(tok[s, where, :], w, preferred_element_type=F32)
                kv[part, s, where, :] = y.astype(BF16)
                return carry

            lax.fori_loop(0, seqs * (span // tile), body, 0)
            pltpu.make_async_copy(
                kv.at[part], (key_out, value_out)[part], out_sem.at[part]
            ).start()

    for k in range(tp_count - 1):
        bias_move(k, lax.rem(tp + tp_count - k - 1, tp_count), tp).wait_recv()
    bias[tp] = bias_all[:, tp]

    row_id = lax.broadcasted_iota(jnp.int32, (rows_h, cols), 0)
    col_id = lax.broadcasted_iota(jnp.int32, (rows_h, cols), 1)
    own = row_id == col_id // head_dim
    q = query[:, pl.ds(col_start, cols)].astype(F32)
    total_heads = offset.shape[1]
    pick = lax.broadcasted_iota(jnp.int32, (rows_h, total_heads), 1) == (
        lax.broadcasted_iota(jnp.int32, (rows_h, total_heads), 0) + tp * heads
    )
    offset_col = jnp.sum(jnp.where(pick, offset[...], 0.0), axis=1, keepdims=True)
    logits = []
    for s in range(seqs):
        q_rows = jnp.where(own, q[s : s + 1], 0.0).astype(BF16)
        b = jnp.concatenate([bias[t, s] for t in range(tp_count)], axis=1)
        bias_out[s] = b
        b = b.astype(F32)
        if rows_h > heads:
            b = jnp.concatenate([b, jnp.zeros((rows_h - heads, span), F32)], axis=0)
        logits.append(
            lax.dot_general(
                q_rows, kv[0, s], (((1,), (1,)), ((), ())), preferred_element_type=F32
            )
            * (head_dim**-0.5)
            + offset_col
            + b
        )
    logits = jnp.concatenate(logits, axis=0)
    soft = jnp.log1p(jnp.exp(-jnp.abs(logits)))
    fading = -jnp.maximum(logits, 0.0) - soft
    taking = jnp.minimum(logits, 0.0) - soft
    high = fading.astype(BF16)
    rest = fading - high.astype(F32)
    mid = rest.astype(BF16)
    low = (rest - mid.astype(F32)).astype(BF16)
    later = (
        lax.broadcasted_iota(jnp.int32, (span, span), 0)
        > lax.broadcasted_iota(jnp.int32, (span, span), 1)
    ).astype(F32).astype(BF16)
    sums = jnp.dot(
        jnp.concatenate([high, mid, low], axis=0), later, preferred_element_type=F32
    )
    m = seqs * rows_h
    within = sums[:m] + sums[m : 2 * m] + sums[2 * m :]
    weights = jnp.exp(taking + within).astype(BF16)
    totals = jnp.sum(fading, axis=1, keepdims=True)
    for s in range(seqs):
        at = slice(s * rows_h, (s + 1) * rows_h)
        partial = jnp.dot(weights[at], kv[1, s], preferred_element_type=F32)
        packed[me, s : s + 1] = jnp.sum(jnp.where(own, partial, 0.0), axis=0, keepdims=True)
        packed[me, seqs + s : seqs + s + 1] = jnp.sum(
            jnp.where(own, totals[at], 0.0), axis=0, keepdims=True
        )

    def mix_move(k, source):
        return pltpu.make_async_remote_copy(
            src_ref=packed.at[source], dst_ref=packed.at[source],
            send_sem=mix_send.at[k - 1], recv_sem=mix_recv.at[k - 1],
            device_id={"sp": lax.rem(me + k, n)}, device_id_type=MESH,
        )

    for k in range(1, n):
        launch(mix_move(k, me))
    for k in range(1, n):
        mix_move(k, lax.rem(me + n - k, n)).wait_recv()
    mixture = jnp.zeros((seqs, cols), F32)
    carry = jnp.zeros((seqs, cols), F32)
    for at in range(n - 1, -1, -1):
        mixture = mixture + jnp.exp(carry) * packed[at, :seqs]
        carry = carry + packed[at, seqs:]
    for s in range(seqs):
        x = mixture[s : s + 1]
        mean = jnp.sum(jnp.where(own, x * x, 0.0), axis=1, keepdims=True) / head_dim
        scale = jnp.sum(jnp.where(own, lax.rsqrt(mean + 1e-06), 0.0), axis=0, keepdims=True)
        reading_out[s : s + 1] = x * scale

    for c in sent_list:
        c.wait_send()
    for part in range(2):
        pltpu.make_async_copy(
            kv.at[part], (key_out, value_out)[part], out_sem.at[part]
        ).wait()


def per_device(tokens, key_weight, value_weight, queries, head_offset, key_bias):
    n, tp_count = lax.axis_size("sp"), lax.axis_size("tp")
    assert n % 2 == 0 and lax.axis_size("gr") == 2
    seqs, pos, width = tokens.shape
    rows, kv_width = key_weight.shape
    head_count = head_offset.shape[0]
    head_dim = kv_width // head_count
    cols = kv_width // tp_count
    heads = head_count // tp_count
    rows_h = max(8, heads)
    span = tp_count * pos
    hops = n // 2
    bias_rows = jnp.transpose(key_bias, (0, 2, 1)).reshape(seqs, tp_count, heads, pos)
    dims = (n, tp_count, seqs, pos, width, rows, cols, heads, head_dim, rows_h)
    peers = max(tp_count - 1, 1)
    chunks = n if (width // n) % 128 == 0 else 1
    dma = pltpu.SemaphoreType.DMA
    key_cache, value_cache, bias_cache, reading = pl.pallas_call(
        functools.partial(kernel, dims),
        out_shape=(
            jax.ShapeDtypeStruct((seqs, span, cols), BF16),
            jax.ShapeDtypeStruct((seqs, span, cols), BF16),
            jax.ShapeDtypeStruct((seqs, heads, span), BF16),
            jax.ShapeDtypeStruct((seqs, cols), F32),
        ),
        in_specs=[pl.BlockSpec(memory_space=pl.ANY)] * 6,
        out_specs=[
            pl.BlockSpec(memory_space=pl.ANY),
            pl.BlockSpec(memory_space=pl.ANY),
            pl.BlockSpec(memory_space=pltpu.VMEM),
            pl.BlockSpec(memory_space=pltpu.VMEM),
        ],
        scratch_shapes=[
            pltpu.VMEM((seqs, span, width), BF16),
            pltpu.VMEM((2, n, rows, cols), BF16),
            pltpu.VMEM((2, seqs, span, cols), F32),
            pltpu.VMEM((2, seqs, span, cols), BF16),
            pltpu.VMEM((tp_count, seqs, heads, pos), BF16),
            pltpu.VMEM(queries.shape, BF16),
            pltpu.VMEM((1, head_count), F32),
            pltpu.VMEM((seqs, tp_count, heads, pos), BF16),
            pltpu.VMEM((n, 2 * seqs, cols), F32),
            dma((6,)),
            dma((2, hops, SUBS)),
            dma((2, hops, SUBS)),
            dma((2, hops, SUBS)),
            dma((2, hops, SUBS)),
            dma((chunks, peers)),
            dma((chunks, peers)),
            dma((peers,)),
            dma((peers,)),
            dma((n - 1,)),
            dma((n - 1,)),
            dma((2,)),
        ],
        compiler_params=pltpu.CompilerParams(collective_id=0, has_side_effects=True),
        name="prefill_read",
    )(tokens, key_weight, value_weight, queries, head_offset.reshape(1, head_count), bias_rows)
    return key_cache, value_cache, jnp.transpose(bias_cache, (0, 2, 1)), reading


def solution(mesh):
    in_specs = (
        P("gr", ("sp", "tp"), None),
        P("sp", None),
        P("sp", None),
        P("gr", None),
        P(),
        P("gr", ("sp", "tp"), None),
    )
    out_specs = (P("gr", "sp", "tp"), P("gr", "sp", "tp"), P("gr", "sp", "tp"), P("gr", "tp"))
    return jax.shard_map(
        per_device, mesh=mesh, in_specs=in_specs, out_specs=out_specs, check_vma=False
    )
```

time: 180 us -> 42.6 us (0.24)
  waiting for transfers between devices: 108 us -> 0 us
  Pallas kernels: 0 us -> 37.8 us
  blocking collectives: 35.7 us -> 0 us
  between operations: 14.2 us -> 0.65 us
  other arithmetic: 6.49 us -> 0 us
  matrix products: 5.64 us -> 0 us
  starting transfers between devices: 4.31 us -> 0 us
    all_gather x2 -> x0, waiting for transfers between devices: 107 us -> none  [the longest x1 77.3 us: per_device(): full_cols = lax.all_gather(own_cols, 'sp', axis=0, tiled=True)]
    pallas_call x0 -> x1, Pallas kernels: none -> 37.8 us  [per_device(): pl.pallas_call(functools.partial(kernel, dims), out_shape=(jax.ShapeDtype...]
    psum x1 -> x0, blocking collectives: 17.9 us -> none  [per_device(): mixture = lax.psum(partial_value, 'sp')]
    all_gather x1 -> x0, blocking collectives: 17.7 us -> none  [carried_in(): everything = lax.all_gather(x, axis)]
    dot_general x3 -> x0, matrix products: 5.64 us -> none  [the longest x1 5.22 us: per_device(): jnp.einsum('spd,dw->spw', lax.all_gather(tokens, 'tp', axis=1, tiled=True...]
    another operation x2 -> x0, other arithmetic: 5.02 us -> none
    all_to_all x1 -> x0, starting transfers between devices: 4.23 us -> none  [per_device(): lax.all_to_all(key_bias, 'tp', split_axis=2, concat_axis=1, tiled=True)]
    unnamed x13 -> x10, local copies, waits for them, and re-layouts: 2.91 us -> 4 us
  transfers between devices with their start and end apart: 3 -> 0, of which waited for: 2 -> 0; matrix products, arithmetic and copies ran while one was open for 5% -> 0% of each run, Pallas kernels for 0% -> 0%
where the time goes in v1:
time: 42.6 us; the launch traced here: 42.4 us
  Pallas kernels  37.8 us (89%)
  local copies, waits for them, and re-layouts  4 us (9%)
  between operations  0.65 us (2%)
    pallas_call x1, Pallas kernels, per_device(): pl.pallas_call(functools.partial(kernel, dims), out_shape=(jax.ShapeDtype...  37.8 us
    unnamed x10, local copies, waits for them, and re-layouts  4 us

profile of v1, /device:TPU:0, one launch (start us, length us, event | category | flops | bytes accessed | tf_op | source)
XLA Modules:
  0.0 42.4 jit_solution(16235387699428002272)
XLA Ops:
  0.6 37.8 %prefill_read.1 = (bf16[2,256,512]{2,1,0:T(8,128)(2,1)}, bf16[2,256,512]{2,1,0:T(8,128)(2,1)}, bf16[2,8,256]{2,1,0:T(8,128)(2,1)}, f32[2,512]{1,0:T(2,128)}) custom-call(bf16[2,128,2048]{2,1,0:T(8,128)(2,1)} %tokens.1, bf16[256,1024]{1,0:T(8,128)(2,1)} %key_weight.1, bf16[256,1024]{1,0:T(8,128)(2,1)} %value_weight.1, bf16[2,1024]{1,0:T(2,128)(2,1)} %queries.1, ...), custom_call_target="tpu_custom_call" | custom-call | tf_op jit(solution)/shard_map/prefill_read/pallas_call | solution.py:328
  38.4 0.0 copy-start
  38.4 1.9 %copy.14 = bf16[2,256,512]{2,1,0:T(8,128)(2,1)} copy(bf16[2,256,512]{2,1,0:T(8,128)(2,1)} %get-tuple-element.16) | data formatting | bytes 1048576
  40.3 0.0 copy-done
  40.3 0.0 copy-start.1
  40.3 0.8 %copy.15 = bf16[2,256,512]{2,1,0:T(8,128)(2,1)} copy(bf16[2,256,512]{2,1,0:T(8,128)(2,1)S(1)} %copy-done) | data formatting | bytes 1048576
  41.1 0.0 copy-done.1
  41.1 0.0 copy-start.2
  41.1 0.6 %copy.16 = bf16[2,256,8]{1,2,0:T(8,128)(2,1)} copy(bf16[2,256,8]{1,2,0:T(8,128)(2,1)S(1)} %bitcast.6) | data formatting | bytes 16384
  41.7 0.1 copy-done.2
  41.8 0.6 %copy.17 = f32[2,512]{1,0:T(2,128)} copy(f32[2,512]{1,0:T(2,128)S(1)} %copy-done.2) | data formatting | bytes 8192
Async XLA Ops:
  38.4 1.9 %copy-start = (bf16[2,256,512]{2,1,0:T(8,128)(2,1)S(1)}, bf16[2,256,512]{2,1,0:T(8,128)(2,1)}, u32[]{:S(2)}) copy-start(bf16[2,256,512]{2,1,0:T(8,128)(2,1)} %get-tuple-element.17) | copy-start | bytes 1572868
  40.3 0.8 %copy-start.1 = (bf16[2,8,256]{2,1,0:T(8,128)(2,1)S(1)}, bf16[2,8,256]{2,1,0:T(8,128)(2,1)}, u32[]{:S(2)}) copy-start(bf16[2,8,256]{2,1,0:T(8,128)(2,1)} %get-tuple-element.10) | copy-start | bytes 24580
  41.1 0.7 %copy-start.2 = (f32[2,512]{1,0:T(2,128)S(1)}, f32[2,512]{1,0:T(2,128)}, u32[]{:S(2)}) copy-start(f32[2,512]{1,0:T(2,128)} %get-tuple-element.19) | copy-start | bytes 12292

commit v2 on v1

--- a/solution.py
+++ b/solution.py
@@ -27,10 +27,10 @@
 def kernel(
     dims,
     tokens, key_weight, value_weight, queries, head_offset, key_bias,
-    key_out, value_out, bias_out, reading_out,
-    tok, wts, acc, kv, bias, query, offset, bias_all, packed,
+    kv, bias_out, packed,
+    tok, wts, acc, bias, query, offset, bias_all,
     local_sem, ring_send, ring_recv, pair_send, pair_recv,
-    tok_send, tok_recv, bias_send, bias_recv, mix_send, mix_recv, out_sem,
+    tok_send, tok_recv, bias_send, bias_recv, mix_send, mix_recv,
 ):
     n, tp_count, seqs, pos, width, rows, cols, heads, head_dim, rows_h = dims
     hops = n // 2
@@ -167,10 +167,6 @@
                 return carry
 
             lax.fori_loop(0, seqs, body, 0)
-            if last:
-                pltpu.make_async_copy(
-                    kv.at[part], (key_out, value_out)[part], out_sem.at[part]
-                ).start()
 
     def pair_ready(hop):
         for direction in range(2):
@@ -218,9 +214,6 @@
                 return carry
 
             lax.fori_loop(0, seqs * (span // tile), body, 0)
-            pltpu.make_async_copy(
-                kv.at[part], (key_out, value_out)[part], out_sem.at[part]
-            ).start()
 
     for k in range(tp_count - 1):
         bias_move(k, lax.rem(tp + tp_count - k - 1, tp_count), tp).wait_recv()
@@ -289,6 +282,23 @@
         launch(mix_move(k, me))
     for k in range(1, n):
         mix_move(k, lax.rem(me + n - k, n)).wait_recv()
+    for c in sent_list:
+        c.wait_send()
+
+
+def finish(n, head_dim, kv, bias, packed, key_out, value_out, bias_out, reading_out, sems):
+    moves = [
+        pltpu.make_async_copy(kv.at[0], key_out, sems.at[0]),
+        pltpu.make_async_copy(kv.at[1], value_out, sems.at[1]),
+        pltpu.make_async_copy(bias, bias_out, sems.at[2]),
+    ]
+    for c in moves:
+        c.start()
+    seqs, cols = reading_out.shape
+    rows_h = max(8, cols // head_dim)
+    row_id = lax.broadcasted_iota(jnp.int32, (rows_h, cols), 0)
+    col_id = lax.broadcasted_iota(jnp.int32, (rows_h, cols), 1)
+    own = row_id == col_id // head_dim
     mixture = jnp.zeros((seqs, cols), F32)
     carry = jnp.zeros((seqs, cols), F32)
     for at in range(n - 1, -1, -1):
@@ -299,13 +309,8 @@
         mean = jnp.sum(jnp.where(own, x * x, 0.0), axis=1, keepdims=True) / head_dim
         scale = jnp.sum(jnp.where(own, lax.rsqrt(mean + 1e-06), 0.0), axis=0, keepdims=True)
         reading_out[s : s + 1] = x * scale
-
-    for c in sent_list:
-        c.wait_send()
-    for part in range(2):
-        pltpu.make_async_copy(
-            kv.at[part], (key_out, value_out)[part], out_sem.at[part]
-        ).wait()
+    for c in moves:
+        c.wait()
 
 
 def per_device(tokens, key_weight, value_weight, queries, head_offset, key_bias):
@@ -325,31 +330,23 @@
     peers = max(tp_count - 1, 1)
     chunks = n if (width // n) % 128 == 0 else 1
     dma = pltpu.SemaphoreType.DMA
-    key_cache, value_cache, bias_cache, reading = pl.pallas_call(
+    kv, bias_held, packed = pl.pallas_call(
         functools.partial(kernel, dims),
         out_shape=(
-            jax.ShapeDtypeStruct((seqs, span, cols), BF16),
-            jax.ShapeDtypeStruct((seqs, span, cols), BF16),
+            jax.ShapeDtypeStruct((2, seqs, span, cols), BF16),
             jax.ShapeDtypeStruct((seqs, heads, span), BF16),
-            jax.ShapeDtypeStruct((seqs, cols), F32),
+            jax.ShapeDtypeStruct((n, 2 * seqs, cols), F32),
         ),
-        in_specs=[pl.BlockSpec(memory_space=pl.ANY)] * 6,
-        out_specs=[
-            pl.BlockSpec(memory_space=pl.ANY),
-            pl.BlockSpec(memory_space=pl.ANY),
-            pl.BlockSpec(memory_space=pltpu.VMEM),
-            pl.BlockSpec(memory_space=pltpu.VMEM),
-        ],
+        in_specs=[pl.BlockSpec(memory_space=pltpu.HBM)] * 6,
+        out_specs=[pl.BlockSpec(memory_space=pltpu.VMEM)] * 3,
         scratch_shapes=[
             pltpu.VMEM((seqs, span, width), BF16),
             pltpu.VMEM((2, n, rows, cols), BF16),
             pltpu.VMEM((2, seqs, span, cols), F32),
-            pltpu.VMEM((2, seqs, span, cols), BF16),
             pltpu.VMEM((tp_count, seqs, heads, pos), BF16),
             pltpu.VMEM(queries.shape, BF16),
             pltpu.VMEM((1, head_count), F32),
             pltpu.VMEM((seqs, tp_count, heads, pos), BF16),
-            pltpu.VMEM((n, 2 * seqs, cols), F32),
             dma((6,)),
             dma((2, hops, SUBS)),
             dma((2, hops, SUBS)),
@@ -361,11 +358,35 @@
             dma((peers,)),
             dma((n - 1,)),
             dma((n - 1,)),
-            dma((2,)),
         ],
-        compiler_params=pltpu.CompilerParams(collective_id=0, has_side_effects=True),
-        name="prefill_read",
-    )(tokens, key_weight, value_weight, queries, head_offset.reshape(1, head_count), bias_rows)
+        compiler_params=pltpu.CompilerParams(
+            collective_id=0, has_side_effects=True, vmem_limit_bytes=36 * 2**20
+        ),
+        name="prefill",
+    )(*(pltpu.with_memory_space_constraint(a, pltpu.HBM) for a in (tokens, key_weight, value_weight, queries, head_offset.reshape(1, head_count), bias_rows)))
+    key_cache, value_cache, bias_cache, reading = pl.pallas_call(
+        functools.partial(finish, n, head_dim),
+        out_shape=(
+            jax.ShapeDtypeStruct((seqs, span, cols), BF16),
+            jax.ShapeDtypeStruct((seqs, span, cols), BF16),
+            jax.ShapeDtypeStruct((seqs, heads, span), BF16),
+            jax.ShapeDtypeStruct((seqs, cols), F32),
+        ),
+        in_specs=[
+            pl.BlockSpec(memory_space=pl.ANY),
+            pl.BlockSpec(memory_space=pl.ANY),
+            pl.BlockSpec(memory_space=pltpu.VMEM),
+        ],
+        out_specs=[
+            pl.BlockSpec(memory_space=pl.ANY),
+            pl.BlockSpec(memory_space=pl.ANY),
+            pl.BlockSpec(memory_space=pl.ANY),
+            pl.BlockSpec(memory_space=pltpu.VMEM),
+        ],
+        scratch_shapes=[dma((3,))],
+        compiler_params=pltpu.CompilerParams(vmem_limit_bytes=4 * 2**20),
+        name="finish",
+    )(kv, bias_held, packed)
     return key_cache, value_cache, jnp.transpose(bias_cache, (0, 2, 1)), reading
 
 

time: 42.6 us -> 39.4 us (0.925)
  local copies, waits for them, and re-layouts: 4 us -> 0 us
  Pallas kernels: 37.8 us -> 38.6 us
    unnamed x10 -> x0, local copies, waits for them, and re-layouts: 4 us -> none
    pallas_call x0 -> x1, Pallas kernels: none -> 1.6 us  [per_device(): pl.pallas_call(functools.partial(finish, n, head_dim), out_shape=(jax.Sha...]
    pallas_call x1, Pallas kernels: 37.8 us -> 37 us  [per_device(): pl.pallas_call(functools.partial(kernel, dims), out_shape=(jax.ShapeDtype...]
where the time goes in v2:
time: 39.4 us; the launch traced here: 39.3 us
  Pallas kernels  38.6 us (98%)
  between operations  0.64 us (2%)
    pallas_call x1, Pallas kernels, per_device(): pl.pallas_call(functools.partial(kernel, dims), out_shape=(jax.ShapeDtype...  37 us
    pallas_call x1, Pallas kernels, per_device(): pl.pallas_call(functools.partial(finish, n, head_dim), out_shape=(jax.Sha...  1.6 us

profile of v2, /device:TPU:0, one launch (start us, length us, event | category | flops | bytes accessed | tf_op | source)
XLA Modules:
  0.0 39.3 jit_solution(3847597987772662588)
XLA Ops:
  0.6 37.0 %prefill.1 = (bf16[2,2,256,512]{3,2,1,0:T(8,128)(2,1)S(1)}, bf16[2,8,256]{2,1,0:T(8,128)(2,1)S(1)}, f32[8,4,512]{2,1,0:T(4,128)S(1)}) custom-call(bf16[2,128,2048]{2,1,0:T(8,128)(2,1)} %tokens.1, bf16[256,1024]{1,0:T(8,128)(2,1)} %key_weight.1, bf16[256,1024]{1,0:T(8,128)(2,1)} %value_weight.1, bf16[2,1024]{1,0:T(2,128)(2,1)} %queries.1, f32[1,16]{1,0:T(1,128)} %bitcast.6, ...), custom_call_target="tpu_custom_call" | custom-call | tf_op jit(solution)/shard_map/prefill/pallas_call | solution.py:333
  37.7 1.6 %finish.1 = (bf16[2,256,512]{2,1,0:T(8,128)(2,1)}, bf16[2,256,512]{2,1,0:T(8,128)(2,1)}, bf16[2,8,256]{2,1,0:T(8,128)(2,1)}, f32[2,512]{1,0:T(2,128)}) custom-call(bf16[2,2,256,512]{3,2,1,0:T(8,128)(2,1)S(1)} %get-tuple-element.11.kv, bf16[2,8,256]{2,1,0:T(8,128)(2,1)S(1)} %get-tuple-element.12.bias, f32[8,4,512]{2,1,0:T(4,128)S(1)} %get-tuple-element.13.packed), custom_call_target="tpu_custom_call" | custom-call | tf_op jit(solution)/shard_map/finish/pallas_call | solution.py:367

commit v3 on v2

--- a/solution.py
+++ b/solution.py
@@ -10,7 +10,7 @@
 MESH = pl.DeviceIdType.MESH
 F32 = jnp.float32
 BF16 = jnp.bfloat16
-SUBS = 2
+SUBS = 4
 
 
 def ring_place(index, length):
@@ -150,7 +150,7 @@
         for k in range(tp_count - 1):
             tok_move(i, k, lax.rem(tp + tp_count - k - 1, tp_count)).wait_recv()
 
-    def multiply(i, last):
+    def multiply(i):
         owner = owner_at(order[i])
         for part in range(2):
             w = wts[part, owner]
@@ -160,13 +160,20 @@
                 y = jnp.dot(x, w, preferred_element_type=F32)
                 if i > 0:
                     y = acc[part, s] + y
-                if last:
-                    kv[part, s] = y.astype(BF16)
-                else:
-                    acc[part, s] = y
+                acc[part, s] = y
                 return carry
 
             lax.fori_loop(0, seqs, body, 0)
+
+    def close(i, source):
+        owner = owner_at(order[i])
+        where = pl.ds(pl.multiple_of(source * pos, pos), pos)
+        for part in range(2):
+            for s in range(seqs):
+                y = jnp.dot(
+                    tok[s, where, tok_columns(i)], wts[part, owner], preferred_element_type=F32
+                )
+                kv[part, s, where, :] = (acc[part, s, where, :] + y).astype(BF16)
 
     def pair_ready(hop):
         for direction in range(2):
@@ -185,8 +192,14 @@
             pair_ready(hop)
         if chunked:
             for i in steps_of_hop(hop):
-                tokens_ready(i)
-                multiply(i, i == len(order) - 1)
+                if i < len(order) - 1:
+                    tokens_ready(i)
+                    multiply(i)
+                else:
+                    close(i, tp)
+                    tokens_ready(i)
+                    for p in tp_peers:
+                        close(i, p)
 
     for hop in range(1, hops + 1):
         for sub in range(SUBS):

time: 39.4 us -> 39 us (0.990)
  Pallas kernels: 38.6 us -> 38.2 us
    pallas_call x1, Pallas kernels: 37 us -> 36.6 us  [per_device(): pl.pallas_call(functools.partial(kernel, dims), out_shape=(jax.ShapeDtype...]
where the time goes in v3:
time: 39 us; the launch traced here: 38.8 us
  Pallas kernels  38.2 us (98%)
  between operations  0.64 us (2%)
    pallas_call x1, Pallas kernels, per_device(): pl.pallas_call(functools.partial(kernel, dims), out_shape=(jax.ShapeDtype...  36.6 us
    pallas_call x1, Pallas kernels, per_device(): pl.pallas_call(functools.partial(finish, n, head_dim), out_shape=(jax.Sha...  1.6 us

profile of v3, /device:TPU:0, one launch (start us, length us, event | category | flops | bytes accessed | tf_op | source)
XLA Modules:
  0.0 38.8 jit_solution(9384247984358644111)
XLA Ops:
  0.6 36.6 %prefill.1 = (bf16[2,2,256,512]{3,2,1,0:T(8,128)(2,1)S(1)}, bf16[2,8,256]{2,1,0:T(8,128)(2,1)S(1)}, f32[8,4,512]{2,1,0:T(4,128)S(1)}) custom-call(bf16[2,128,2048]{2,1,0:T(8,128)(2,1)} %tokens.1, bf16[256,1024]{1,0:T(8,128)(2,1)} %key_weight.1, bf16[256,1024]{1,0:T(8,128)(2,1)} %value_weight.1, bf16[2,1024]{1,0:T(2,128)(2,1)} %queries.1, f32[1,16]{1,0:T(1,128)} %bitcast.6, ...), custom_call_target="tpu_custom_call" | custom-call | tf_op jit(solution)/shard_map/prefill/pallas_call | solution.py:346
  37.2 1.6 %finish.1 = (bf16[2,256,512]{2,1,0:T(8,128)(2,1)}, bf16[2,256,512]{2,1,0:T(8,128)(2,1)}, bf16[2,8,256]{2,1,0:T(8,128)(2,1)}, f32[2,512]{1,0:T(2,128)}) custom-call(bf16[2,2,256,512]{3,2,1,0:T(8,128)(2,1)S(1)} %get-tuple-element.11.kv, bf16[2,8,256]{2,1,0:T(8,128)(2,1)S(1)} %get-tuple-element.12.bias, f32[8,4,512]{2,1,0:T(4,128)S(1)} %get-tuple-element.13.packed), custom_call_target="tpu_custom_call" | custom-call | tf_op jit(solution)/shard_map/finish/pallas_call | solution.py:380
